TPU v7x, 32 devices: a whole 2x2x4 slice. The times are simulated.
32 devices in a mesh: grp: 2 (over x), ep: 8 (over z, y), tp: 2 (over core).
Axes of the slice: x: 2, y: 2, z: 4, core: 2. Of those that a mesh axis runs over, the one named last changes fastest.
Arguments:
- tokens: bfloat16 [4096, 2048], P(('grp', 'ep', 'tp')), parts along dimension 0, may hold values from -6 to 6
- norm_gain: float32 [2048], replicated, may hold values from 0.1 to 1.9
- expert_ids: int32 [4096, 2], P(('grp', 'ep', 'tp')), parts along dimension 0, may hold values from 0 to 7, as said below
- gate_weights: float32 [4096, 2], P(('grp', 'ep', 'tp')), parts along dimension 0, may hold values from 0.1 to 1
- w_gate: bfloat16 [8, 2048, 512], P('ep', None, 'tp'), may hold values from -0.125 to 0.125
- w_up: bfloat16 [8, 2048, 512], P('ep', None, 'tp'), may hold values from -0.125 to 0.125
- w_down: bfloat16 [8, 512, 2048], P('ep', 'tp'), may hold values from -0.25 to 0.25
Outputs:
- mixed: bfloat16 [4096, 2048], P(('grp', 'ep', 'tp')), parts along dimension 0
There are 2 independent parts, one for each index of `grp`. A program takes and returns all parts, laid end to end along the dimension named above; an argument that names none is the same for every part. Nothing has to cross between parts.
Inputs may be any that keep to these rules, and one draw needn't show every extreme that they name: `expert_ids`: the 2 experts of a token are different and lie in one group of 2 consecutive experts. Among the rows of one device (aligned blocks of 128 rows) no expert is named more than 64 times, and in every such block some expert is named exactly 64 times.
All inputs are finite; a program needn't handle non-finite values.
Results may differ from a plain program's by a relative error of at most 0.0078.
Values may be sent and summed in bfloat16 or wider, within the bound.
A program may use at most 64 MiB of HBM per device.

v0:
```python
import jax
import jax.numpy as jnp
from jax import lax
from jax.sharding import PartitionSpec as P

N_GROUPS = 4


def normalize(tokens, norm_gain):
    values = tokens.astype(jnp.float32)
    scaled = values * lax.rsqrt(jnp.mean(values * values, axis=-1, keepdims=True) + 1e-06)
    return (scaled * norm_gain).astype(jnp.bfloat16)


def expert_whole(bucket_rows, full_gate, full_up, full_down, blocks):
    gate_act = jnp.einsum(
        "secd,edf->secf", bucket_rows, full_gate, preferred_element_type=jnp.float32
    )
    up_act = jnp.einsum("secd,edf->secf", bucket_rows, full_up, preferred_element_type=jnp.float32)
    hidden = (jax.nn.silu(gate_act) * up_act).astype(jnp.bfloat16)
    width = hidden.shape[-1] // blocks
    total = jnp.zeros(bucket_rows.shape, jnp.float32)
    for index in range(blocks):
        partial_value = jnp.einsum(
            "secf,efd->secd",
            hidden[..., index * width : (index + 1) * width],
            full_down[:, index * width : (index + 1) * width, :],
            preferred_element_type=jnp.float32,
        )
        rounded = lax.optimization_barrier(partial_value.astype(jnp.bfloat16))
        total = total + rounded.astype(jnp.float32)
    return total.astype(jnp.bfloat16)


def shards(tokens, norm_gain, expert_ids, gate_weights, w_gate, w_up, w_down):
    normed = normalize(tokens, norm_gain)
    n_tok, model_width = normed.shape
    top_count = expert_ids.shape[1]
    local_experts = w_gate.shape[0]
    n_ep = lax.axis_size("ep")
    n_tp = lax.axis_size("tp")
    n_exp = local_experts * n_ep
    capacity = top_count * (n_tok // 2) // (n_exp // N_GROUPS)
    total = n_tok * top_count
    n_slots = n_exp * capacity
    flat_e = expert_ids.reshape(-1)
    onehot = (flat_e[:, None] == jnp.arange(n_exp, dtype=jnp.int32)[None, :]).astype(jnp.bfloat16)
    positions = jnp.arange(total, dtype=jnp.int32)
    earlier = (positions[:, None] > positions[None, :]).astype(jnp.bfloat16)
    before = jnp.dot(earlier, onehot, preferred_element_type=jnp.float32)
    slot_index = jnp.sum(before * onehot.astype(jnp.float32), axis=1).astype(jnp.int32)
    dest_index = flat_e * capacity + slot_index
    slot_ids = jnp.arange(n_slots, dtype=jnp.int32)
    dispatch = (dest_index[None, :] == slot_ids[:, None]).astype(jnp.bfloat16)
    dispatch_tok = jnp.sum(dispatch.reshape(n_slots, n_tok, top_count), axis=2)
    buckets = jnp.dot(dispatch_tok, normed, preferred_element_type=jnp.float32).astype(jnp.bfloat16)
    buckets = buckets.reshape(n_exp, capacity, model_width)
    full_gate, full_up, full_down = (
        lax.all_gather(w_gate, "tp", axis=2, tiled=True),
        lax.all_gather(w_up, "tp", axis=2, tiled=True),
        lax.all_gather(w_down, "tp", axis=1, tiled=True),
    )
    received = lax.all_to_all(buckets, "ep", split_axis=0, concat_axis=0, tiled=True)
    grouped_rows = received.reshape(-1, local_experts, received.shape[1], model_width)
    computed = expert_whole(grouped_rows, full_gate, full_up, full_down, n_tp).reshape(
        received.shape
    )
    results = lax.all_to_all(computed, "ep", split_axis=0, concat_axis=0, tiled=True)
    results = results.reshape(n_slots, model_width)
    dest_pairs = dest_index.reshape(n_tok, top_count)
    mixed = jnp.zeros((n_tok, model_width), jnp.float32)
    for index in range(top_count):
        select = (dest_pairs[:, index][:, None] == slot_ids[None, :]).astype(jnp.bfloat16)
        picked = jnp.dot(select, results, preferred_element_type=jnp.float32)
        mixed = mixed + picked * gate_weights[:, index][:, None]
    return mixed.astype(jnp.bfloat16)


def solution(mesh):
    placed = (
        P(("grp", "ep", "tp"), None),
        P(),
        P(("grp", "ep", "tp"), None),
        P(("grp", "ep", "tp"), None),
        P("ep", None, "tp"),
        P("ep", None, "tp"),
        P("ep", "tp", None),
    )
    return jax.shard_map(
        shards, mesh=mesh, in_specs=placed, out_specs=P(("grp", "ep", "tp"), None), check_vma=False
    )
```

profile of v0, /device:TPU:0, one launch (start us, length us, event | category | flops | bytes accessed | tf_op | source)
XLA Modules:
  0.0 141.7 jit_solution(16173483289323358371)
XLA Ops:
  6.5 0.0 all-gather.4.cloned.1.call-start
  6.5 0.7 all-gather.4.cloned.1.call-update
  7.3 0.8 copy.19
  8.0 0.1 eq.59
  8.2 0.2 fusion.21
  8.4 0.1 convert_element_type.77
  8.5 0.1 copy.20
  8.6 0.7 multiply_add_fusion
  9.3 0.1 fusion.29
  9.4 1.2 fusion.22
  10.6 0.0 copy-done.1
  10.6 2.9 %convolution_convert_fusion.2 = bf16[512,2048]{1,0:T(8,128)(2,1)} fusion(bf16[512,128]{1,0:T(8,128)(2,1)S(1)} %fusion.29, bf16[128,2048]{1,0:T(8,128)(2,1)S(1)} %copy-done.1, f32[2048]{0:T(1024)} %param.8, f32[128]{0:T(128)S(1)} %add_rsqrt_fusion), kind=kOutput, calls=%fused_computation.3 | convolution fusion | flops 270532608 | bytes 2761216 | tf_op jit(solution)/shard_map/dot_general | solution.py:56
  13.5 7.3 %all-to-all-start = ((bf16[8,64,2048]{2,1,0:T(8,128)(2,1)}), bf16[8,64,2048]{2,1,0:T(8,128)(2,1)S(1)}, u32[]{:S(2)}, u32[]{:S(2)}) async-start(bf16[8,64,2048]{2,1,0:T(8,128)(2,1)} %bitcast.1), calls=%async_computation | async-start | bytes 4194304 | tf_op jit(solution)/shard_map/all_to_all | solution.py:63
  20.8 0.0 all-gather.6.cloned.1.call-start
  20.8 0.7 all-gather.6.cloned.1.call-update
  21.5 0.0 all-gather.8.cloned.1.call-start
  21.6 0.7 all-gather.8.cloned.1.call-update
  22.3 0.0 all-gather.4.cloned.1.call-done
  22.3 46.7 %all-to-all-done = bf16[8,64,2048]{2,1,0:T(8,128)(2,1)S(1)} async-done(((bf16[8,64,2048]{2,1,0:T(8,128)(2,1)}), bf16[8,64,2048]{2,1,0:T(8,128)(2,1)S(1)}, u32[]{:S(2)}, u32[]{:S(2)}) %all-to-all-start) | async-done | bytes 2097184 | tf_op jit(solution)/shard_map/all_to_all | solution.py:63
  69.0 3.8 %fusion.9 = f32[8,1,64,512]{3,2,0,1:T(8,128)} fusion(bf16[8,64,2048]{2,1,0:T(8,128)(2,1)S(1)} %all-to-all-done, bf16[1,2048,512]{2,1,0:T(8,128)(2,1)} %all-gather.4.cloned.1.call-done), kind=kOutput, calls=%fused_computation.15 | convolution fusion | flops 1073741824 | bytes 5242880 | tf_op jit(solution)/shard_map/secd,edf->secf/dot_general | solution.py:16
  72.9 3.2 %fusion.18 = bf16[8,1,64,512]{3,2,0,1:T(8,128)(2,1)S(1)} fusion(bf16[8,64,2048]{2,1,0:T(8,128)(2,1)S(1)} %all-to-all-done, bf16[1,2048,512]{2,1,0:T(8,128)(2,1)} %all-gather.6.cloned.1.call-done, f32[8,1,64,512]{3,2,0,1:T(8,128)} %fusion.9), kind=kOutput, calls=%fused_computation.20 | convolution fusion | flops 1075314688 | bytes 5767168 | tf_op jit(solution)/shard_map/secd,edf->secf/dot_general | solution.py:19
  76.1 0.0 all-gather.8.cloned.1.call-done
  76.1 0.0 copy-start
  76.1 2.1 %fusion = bf16[8,1,64,2048]{3,2,0,1:T(8,128)(2,1)S(1)} fusion(bf16[1,512,2048]{2,1,0:T(8,128)(2,1)} %all-gather.8.cloned.1.call-done, bf16[8,1,64,512]{3,2,0,1:T(8,128)(2,1)S(1)} %fusion.18), kind=kOutput, calls=%fused_computation.4 | convolution fusion | flops 537919488 | bytes 3407872 | tf_op jit(solution)/shard_map/secf,efd->secd/dot_general | solution.py:24
  78.2 0.0 copy-done
  78.2 0.7 fusion.1
  79.0 2.2 %fusion.4 = bf16[8,64,2048]{2,1,0:T(8,128)(2,1)} fusion(bf16[8,1,64,2048]{3,2,0,1:T(8,128)(2,1)S(1)} %fusion.1, bf16[8,1,64,2048]{3,2,0,1:T(8,128)(2,1)S(1)} %fusion), kind=kLoop, calls=%fused_computation.10 | loop fusion | flops 4194304 | bytes 6291456 | tf_op jit(solution)/shard_map/reshape | solution.py:65
  81.1 3.8 %all-to-all-start.1 = ((bf16[8,64,2048]{2,1,0:T(8,128)(2,1)}), bf16[8,64,2048]{2,1,0:T(8,128)(2,1)S(1)}, u32[]{:S(2)}, u32[]{:S(2)}) async-start(bf16[8,64,2048]{2,1,0:T(8,128)(2,1)} %fusion.4), calls=%async_computation.1 | async-start | bytes 4194304 | tf_op jit(solution)/shard_map/all_to_all | solution.py:68
  84.9 0.0 copy-done.2
  84.9 48.4 %all-to-all-done.1 = bf16[8,64,2048]{2,1,0:T(8,128)(2,1)S(1)} async-done(((bf16[8,64,2048]{2,1,0:T(8,128)(2,1)}), bf16[8,64,2048]{2,1,0:T(8,128)(2,1)S(1)}, u32[]{:S(2)}, u32[]{:S(2)}) %all-to-all-start.1) | async-done | bytes 2097184 | tf_op jit(solution)/shard_map/all_to_all | solution.py:68
  133.3 0.5 convolution_multiply_fusion.1
  133.8 1.3 fusion.3
  (7 shorter events, 0.0 us)
Async XLA Ops:
  6.5 4.1 %copy-start.1 = (bf16[128,2048]{1,0:T(8,128)(2,1)S(1)}, bf16[128,2048]{1,0:T(8,128)(2,1)}, u32[]{:S(2)}) copy-start(bf16[128,2048]{1,0:T(8,128)(2,1)} %param.7) | copy-start | bytes 1572868
  6.5 15.8 %all-gather.4.cloned.1.call-start = ((), (), s32[]{:S(2)}) async-start(), calls=%async_computation.2 | async-start | bytes 3145728 | tf_op jit(solution)/shard_map/all_gather | solution.py:59
  13.5 55.5 %all-to-all-start = ((bf16[8,64,2048]{2,1,0:T(8,128)(2,1)}), bf16[8,64,2048]{2,1,0:T(8,128)(2,1)S(1)}, u32[]{:S(2)}, u32[]{:S(2)}) async-start(bf16[8,64,2048]{2,1,0:T(8,128)(2,1)} %bitcast.1), calls=%async_computation | async-start | bytes 4194304 | tf_op jit(solution)/shard_map/all_to_all | solution.py:63
  20.8 52.1 %all-gather.6.cloned.1.call-start = ((), (), s32[]{:S(2)}) async-start(), calls=%async_computation.3 | async-start | bytes 3145728 | tf_op jit(solution)/shard_map/all_gather | solution.py:60
  21.5 54.6 %all-gather.8.cloned.1.call-start = ((), (), s32[]{:S(2)}) async-start(), calls=%async_computation.4 | async-start | bytes 3145728 | tf_op jit(solution)/shard_map/all_gather | solution.py:61
  76.1 2.1 %copy-start = (bf16[1,512,2048]{2,1,0:T(8,128)(2,1)S(1)}, bf16[1,512,2048]{2,1,0:T(8,128)(2,1)}, u32[]{:S(2)}) copy-start(bf16[1,512,2048]{2,1,0:T(8,128)(2,1)} %all-gather.8.cloned.1.call-done) | copy-start | bytes 6291460
  81.1 3.8 %copy-start.2 = (f32[128,2]{0,1:T(2,128)S(1)}, f32[128,2]{0,1:T(2,128)}, u32[]{:S(2)}) copy-start(f32[128,2]{0,1:T(2,128)} %param.10) | copy-start | bytes 3076
  81.1 52.2 %all-to-all-start.1 = ((bf16[8,64,2048]{2,1,0:T(8,128)(2,1)}), bf16[8,64,2048]{2,1,0:T(8,128)(2,1)S(1)}, u32[]{:S(2)}, u32[]{:S(2)}) async-start(bf16[8,64,2048]{2,1,0:T(8,128)(2,1)} %fusion.4), calls=%async_computation.1 | async-start | bytes 4194304 | tf_op jit(solution)/shard_map/all_to_all | solution.py:68
Sparse Core Ops, SparseCore 0:
  8.9 12.8 all-gather.3
  23.3 11.3 all-gather.5
  36.2 11.7 all-gather.7
where the time goes:
time: 142 us
  waiting for transfers between devices  97.2 us (68%)
  matrix products  14.7 us (10%)
  between operations  13.2 us (9%)
  starting transfers between devices  11.1 us (8%)
  other arithmetic  4.17 us (3%)
    all_to_all x1, waiting for transfers between devices, shards(): lax.all_to_all(computed, 'ep', split_axis=0, concat_axis=0, tiled=True)  48.4 us
    all_to_all x1, waiting for transfers between devices, shards(): lax.all_to_all(buckets, 'ep', split_axis=0, concat_axis=0, tiled=True)  46.7 us
    all_to_all x1, starting transfers between devices, shards(): lax.all_to_all(buckets, 'ep', split_axis=0, concat_axis=0, tiled=True)  7.31 us
    dot_general x1, matrix products, expert_whole(): jnp.einsum('secd,edf->secf', bucket_rows, full_gate, preferred_element_ty...  3.84 us
    all_to_all x1, starting transfers between devices, shards(): lax.all_to_all(computed, 'ep', split_axis=0, concat_axis=0, tiled=True)  3.76 us
    dot_general x1, matrix products, expert_whole(): jnp.einsum('secd,edf->secf', bucket_rows, full_up, preferred_element_type...  3.19 us
    dot_general x1, matrix products, shards(): jnp.dot(dispatch_tok, normed, preferred_element_type=jnp.float32)  2.85 us
  transfers between devices with their start and end apart: 5, of which 2 were waited for; matrix products, arithmetic and copies ran while one was open for 9% of the time, Pallas kernels for 0%

commit v1 on v0

--- a/solution.py
+++ b/solution.py
@@ -1,6 +1,10 @@
+import functools
+
 import jax
 import jax.numpy as jnp
 from jax import lax
+from jax.experimental import pallas as pl
+from jax.experimental.pallas import tpu as pltpu
 from jax.sharding import PartitionSpec as P
 
 N_GROUPS = 4
@@ -32,7 +36,7 @@
     return total.astype(jnp.bfloat16)
 
 
-def shards(tokens, norm_gain, expert_ids, gate_weights, w_gate, w_up, w_down):
+def generic_shards(tokens, norm_gain, expert_ids, gate_weights, w_gate, w_up, w_down):
     normed = normalize(tokens, norm_gain)
     n_tok, model_width = normed.shape
     top_count = expert_ids.shape[1]
@@ -76,6 +80,277 @@
     return mixed.astype(jnp.bfloat16)
 
 
+LANES = 128
+MESH = pl.DeviceIdType.MESH
+
+
+def route_order(n_groups, home):
+    low = (home < n_groups // 2).astype(jnp.int32)
+    order = [home]
+    for index in range(n_groups - 1):
+        up = index + (index >= home).astype(jnp.int32)
+        down = n_groups - 1 - index - (index >= n_groups - 1 - home).astype(jnp.int32)
+        order.append(low * up + (1 - low) * down)
+    return order
+
+
+def layer_kernel(
+    n_groups, rows, tok_ref, gain_ref, ids_ref, gates_ref, gate_hbm, up_hbm, down_hbm, out_ref,
+    sent, inbox, own, other, from_pair, back, final, gate_w, up_w, down_w, place,
+    local_sem, w_send, w_recv, z_send, z_recv, y_send, y_recv, p_send, p_recv, b_send, b_recv,
+):
+    n_tok, width = tok_ref.shape
+    half = gate_w.shape[2]
+    members = 2
+    ep = lax.axis_index("ep")
+    core = lax.axis_index("tp")
+    home = ep // members
+    member = ep % members
+    pair_id = {"ep": home * members + 1 - member}
+    core_id = {"tp": 1 - core}
+    order = route_order(n_groups, home)
+
+    def row_id(group):
+        return {"ep": group * members + member}
+
+    locals_ = []
+    for index, (src, dst) in enumerate(((gate_hbm, gate_w), (up_hbm, up_w), (down_hbm, down_w))):
+        copy = pltpu.make_async_copy(src.at[0], dst.at[core], local_sem.at[index])
+        copy.start()
+        locals_.append(copy)
+
+    barrier = pltpu.get_barrier_semaphore()
+    for group in order[1:]:
+        pl.semaphore_signal(barrier, inc=1, device_id=row_id(group), device_id_type=MESH)
+    pl.semaphore_signal(barrier, inc=1, device_id=pair_id, device_id_type=MESH)
+    pl.semaphore_signal(barrier, inc=1, device_id=core_id, device_id_type=MESH)
+
+    ids = ids_ref[...]
+    gates = gates_ref[...]
+    group_of = ids[:, 0:1] // members
+    lane = lax.broadcasted_iota(jnp.int32, (n_tok, LANES), 1)
+    onehot = (group_of == lane).astype(jnp.float32)
+    token = lax.broadcasted_iota(jnp.int32, (n_tok, n_tok), 0)
+    earlier = (token > lax.broadcasted_iota(jnp.int32, (n_tok, n_tok), 1)).astype(jnp.bfloat16)
+    before = jnp.dot(earlier, onehot.astype(jnp.bfloat16), preferred_element_type=jnp.float32)
+    rank = jnp.sum(before * onehot, axis=1, keepdims=True).astype(jnp.int32)
+    slot = group_of * rows + rank
+    slots = lax.broadcasted_iota(jnp.int32, (n_tok, n_groups * rows), 1)
+    place_t = (slot == slots).astype(jnp.float32)
+    place[...] = place_t.astype(jnp.bfloat16)
+    pick = place_t.T.astype(jnp.bfloat16)
+
+    values = tok_ref[...].astype(jnp.float32)
+    scale = lax.rsqrt(jnp.mean(values * values, axis=-1, keepdims=True) + 1e-06)
+    normed = (values * scale * gain_ref[...]).astype(jnp.bfloat16)
+
+    first = (ids[:, 0:1] % members) == 0
+    by_member = (
+        jnp.where(first, gates[:, 0:1], gates[:, 1:2]),
+        jnp.where(first, gates[:, 1:2], gates[:, 0:1]),
+    )
+    extra = jnp.zeros((n_tok, LANES), jnp.float32)
+    for index, weight in enumerate(by_member):
+        left = weight
+        for piece in range(3):
+            part = left.astype(jnp.bfloat16).astype(jnp.float32)
+            extra = jnp.where(lane == index * 3 + piece, part, extra)
+            left = left - part
+    extra = extra.astype(jnp.bfloat16)
+
+    for group in range(n_groups):
+        chosen = pick[group * rows : (group + 1) * rows, :]
+        sent[group, :, :width] = jnp.dot(
+            chosen, normed, preferred_element_type=jnp.float32
+        ).astype(jnp.bfloat16)
+        sent[group, :, width:] = jnp.dot(
+            chosen, extra, preferred_element_type=jnp.float32
+        ).astype(jnp.bfloat16)
+
+    pl.semaphore_wait(barrier, n_groups + 1)
+
+    def z_copy(index):
+        return pltpu.make_async_remote_copy(
+            src_ref=sent.at[order[index]],
+            dst_ref=inbox.at[home, pl.ds(0, rows)],
+            send_sem=z_send.at[index],
+            recv_sem=z_recv.at[home],
+            device_id=row_id(order[index]),
+            device_id_type=MESH,
+        )
+
+    def z_arrival(index):
+        return pltpu.make_async_remote_copy(
+            src_ref=sent.at[order[index]],
+            dst_ref=inbox.at[order[index], pl.ds(0, rows)],
+            send_sem=z_send.at[index],
+            recv_sem=z_recv.at[order[index]],
+            device_id=row_id(order[index]),
+            device_id_type=MESH,
+        )
+
+    def y_copy(index):
+        src = sent.at[home] if index == 0 else inbox.at[order[index], pl.ds(0, rows)]
+        return pltpu.make_async_remote_copy(
+            src_ref=src,
+            dst_ref=inbox.at[order[index], pl.ds(rows, rows)],
+            send_sem=y_send.at[index],
+            recv_sem=y_recv.at[index],
+            device_id=pair_id,
+            device_id_type=MESH,
+        )
+
+    def pair_copy(index):
+        return pltpu.make_async_remote_copy(
+            src_ref=other.at[index],
+            dst_ref=from_pair.at[index],
+            send_sem=p_send.at[index],
+            recv_sem=p_recv.at[index],
+            device_id=pair_id,
+            device_id_type=MESH,
+        )
+
+    def back_copy(index):
+        return pltpu.make_async_remote_copy(
+            src_ref=back.at[index],
+            dst_ref=final.at[home],
+            send_sem=b_send.at[index],
+            recv_sem=b_recv.at[home],
+            device_id=row_id(order[index]),
+            device_id_type=MESH,
+        )
+
+    def back_arrival(index):
+        return pltpu.make_async_remote_copy(
+            src_ref=back.at[index],
+            dst_ref=final.at[order[index]],
+            send_sem=b_send.at[index],
+            recv_sem=b_recv.at[order[index]],
+            device_id=row_id(order[index]),
+            device_id_type=MESH,
+        )
+
+    for index in range(1, n_groups):
+        z_copy(index).start()
+    y_copy(0).start()
+    shared = []
+    for index, (src, dst) in enumerate(((gate_hbm, gate_w), (up_hbm, up_w), (down_hbm, down_w))):
+        copy = pltpu.make_async_remote_copy(
+            src_ref=src.at[0],
+            dst_ref=dst.at[core],
+            send_sem=w_send.at[index],
+            recv_sem=w_recv.at[index],
+            device_id=core_id,
+            device_id_type=MESH,
+        )
+        copy.start()
+        shared.append(copy)
+    inbox[home, 0:rows, :] = sent[home]
+    for copy in locals_:
+        copy.wait()
+    for copy in shared:
+        copy.wait()
+
+    def forward(index):
+        z_arrival(index).wait_recv()
+        y_copy(index).start()
+
+    def compute(index):
+        y_copy(index).wait_recv()
+        group = order[index]
+        x = inbox[group, :, :width]
+        tail = inbox[group, :, width:].astype(jnp.float32)
+        weights = [tail[:, k * 3 : k * 3 + 1] + tail[:, k * 3 + 1 : k * 3 + 2] + tail[:, k * 3 + 2 : k * 3 + 3] for k in range(2)]
+        weight = jnp.where(member == 0, weights[0], weights[1])
+        hidden = []
+        for j in range(2):
+            g = jnp.dot(x, gate_w[j], preferred_element_type=jnp.float32)
+            u = jnp.dot(x, up_w[j], preferred_element_type=jnp.float32)
+            hidden.append((g / (1.0 + jnp.exp(-g)) * u).astype(jnp.bfloat16))
+        step = min(512, width)
+        for begin in range(0, width, step):
+            out = jnp.dot(
+                hidden[0], down_w[0, :, begin : begin + step], preferred_element_type=jnp.float32
+            ) + jnp.dot(
+                hidden[1], down_w[1, :, begin : begin + step], preferred_element_type=jnp.float32
+            )
+            out = out * weight
+            own[index, :, begin : begin + step] = out[:rows]
+            other[index, :, begin : begin + step] = out[rows:].astype(jnp.bfloat16)
+        pair_copy(index).start()
+
+    def combine(index):
+        pair_copy(index).wait_recv()
+        total = (own[index] + from_pair[index].astype(jnp.float32)).astype(jnp.bfloat16)
+        if index == 0:
+            final[home] = total
+        else:
+            back[index] = total
+            back_copy(index).start()
+
+    forward(1)
+    compute(0)
+    for index in range(2, n_groups):
+        forward(index)
+        compute(index - 1)
+        combine(index - 2)
+    compute(n_groups - 1)
+    combine(n_groups - 2)
+    combine(n_groups - 1)
+    for index in range(1, n_groups):
+        back_arrival(index).wait_recv()
+    mixed = jnp.dot(
+        place[...], final[...].reshape(n_groups * rows, width), preferred_element_type=jnp.float32
+    )
+    out_ref[...] = mixed.astype(out_ref.dtype)
+    for index in range(n_groups):
+        if index:
+            z_copy(index).wait_send()
+            back_copy(index).wait_send()
+        y_copy(index).wait_send()
+        pair_copy(index).wait_send()
+
+
+def shards(tokens, norm_gain, expert_ids, gate_weights, w_gate, w_up, w_down):
+    n_tok, width = tokens.shape
+    local_experts = w_gate.shape[0]
+    n_exp = local_experts * lax.axis_size("ep")
+    per_group = n_exp // N_GROUPS
+    top_count = expert_ids.shape[1]
+    if not (local_experts == 1 and per_group == 2 and top_count == 2 and lax.axis_size("tp") == 2):
+        return generic_shards(tokens, norm_gain, expert_ids, gate_weights, w_gate, w_up, w_down)
+    rows = n_tok // 2
+    half = w_gate.shape[2]
+    bf16, f32 = jnp.bfloat16, jnp.float32
+    dma = pltpu.SemaphoreType.DMA
+    vmem = pl.BlockSpec(memory_space=pltpu.VMEM)
+    hbm = pl.BlockSpec(memory_space=pl.ANY)
+    return pl.pallas_call(
+        functools.partial(layer_kernel, N_GROUPS, rows),
+        out_shape=jax.ShapeDtypeStruct((n_tok, width), bf16),
+        in_specs=[vmem] * 4 + [hbm] * 3,
+        out_specs=vmem,
+        scratch_shapes=[
+            pltpu.VMEM((N_GROUPS, rows, width + LANES), bf16),
+            pltpu.VMEM((N_GROUPS, 2 * rows, width + LANES), bf16),
+            pltpu.VMEM((N_GROUPS, rows, width), f32),
+            pltpu.VMEM((N_GROUPS, rows, width), bf16),
+            pltpu.VMEM((N_GROUPS, rows, width), bf16),
+            pltpu.VMEM((N_GROUPS, rows, width), bf16),
+            pltpu.VMEM((N_GROUPS, rows, width), bf16),
+            pltpu.VMEM((2, width, half), bf16),
+            pltpu.VMEM((2, width, half), bf16),
+            pltpu.VMEM((2, half, width), bf16),
+            pltpu.VMEM((n_tok, N_GROUPS * rows), bf16),
+            dma((3,)), dma((3,)), dma((3,)),
+        ] + [dma((N_GROUPS,))] * 8,
+        compiler_params=pltpu.CompilerParams(
+            collective_id=0, has_side_effects=True, vmem_limit_bytes=48 * 1024 * 1024
+        ),
+        name="expert_layer",
+    )(tokens, norm_gain.reshape(1, width), expert_ids, gate_weights, w_gate, w_up, w_down)
+
+
 def solution(mesh):
     placed = (
         P(("grp", "ep", "tp"), None),

time: 142 us -> 81.6 us (0.57)
  waiting for transfers between devices: 97.2 us -> 0 us
  Pallas kernels: 0 us -> 73.7 us
  matrix products: 14.7 us -> 0 us
  between operations: 13.2 us -> 0.02 us
  starting transfers between devices: 11.1 us -> 0 us
  local copies, waits for them, and re-layouts: 1.14 us -> 7.56 us
  other arithmetic: 4.17 us -> 0 us
    all_to_all x2 -> x0, waiting for transfers between devices: 95.1 us -> none  [the longest x1 48.4 us: shards(): lax.all_to_all(computed, 'ep', split_axis=0, concat_axis=0, tiled=True)]
    pallas_call x0 -> x1, Pallas kernels: none -> 73.7 us  [shards(): pl.pallas_call(functools.partial(layer_kernel, N_GROUPS, rows), out_shape...]
    dot_general x8 -> x0, matrix products: 14.7 us -> none  [the longest x1 3.84 us: expert_whole(): jnp.einsum('secd,edf->secf', bucket_rows, full_gate, preferred_element_ty...]
    all_to_all x2 -> x0, starting transfers between devices: 11.1 us -> none  [the longest x1 7.31 us: shards(): lax.all_to_all(buckets, 'ep', split_axis=0, concat_axis=0, tiled=True)]
    unnamed x7 -> x17, local copies, waits for them, and re-layouts: 0.8 us -> 7.56 us
    reshape x1 -> x0, other arithmetic: 2.16 us -> none  [shards(): expert_whole(grouped_rows, full_gate, full_up, full_down, n_tp)]
    unnamed x3 -> x0, waiting for transfers between devices: 2.09 us -> none
  transfers between devices with their start and end apart: 5 -> 0, of which waited for: 2 -> 0; matrix products, arithmetic and copies ran while one was open for 9% -> 0% of each run, Pallas kernels for 0% -> 0%
where the time goes in v1:
time: 81.6 us; the launch traced here: 81.2 us
  Pallas kernels  73.7 us (90%)
  local copies, waits for them, and re-layouts  7.56 us (9%)
    pallas_call x1, Pallas kernels, shards(): pl.pallas_call(functools.partial(layer_kernel, N_GROUPS, rows), out_shape...  73.7 us
    unnamed x17, local copies, waits for them, and re-layouts  7.56 us

profile of v1, /device:TPU:0, one launch (start us, length us, event | category | flops | bytes accessed | tf_op | source)
XLA Modules:
  0.0 81.2 jit_solution(4660997447423258127)
XLA Ops:
  0.0 0.0 copy-start.5
  0.0 0.7 copy-done.5
  0.7 0.0 copy-start.6
  0.7 0.1 copy.8.ids_ref
  0.8 0.6 copy-done.6
  1.4 0.0 copy-start.4
  1.4 0.1 copy.9.gates_ref
  1.5 0.6 copy-done.4
  2.1 0.0 copy-start
  2.1 1.2 %copy-done = bf16[1,2048,256]{2,1,0:T(8,128)(2,1)S(1)} copy-done((bf16[1,2048,256]{2,1,0:T(8,128)(2,1)S(1)}, bf16[1,2048,256]{2,1,0:T(8,128)(2,1)}, u32[]{:S(2)}) %copy-start) | copy-done | bytes 1048600
  3.3 0.0 copy-start.1
  3.3 1.2 %copy-done.1 = bf16[1,2048,256]{2,1,0:T(8,128)(2,1)S(1)} copy-done((bf16[1,2048,256]{2,1,0:T(8,128)(2,1)S(1)}, bf16[1,2048,256]{2,1,0:T(8,128)(2,1)}, u32[]{:S(2)}) %copy-start.1) | copy-done | bytes 1048600
  4.5 0.0 copy-start.2
  4.5 1.2 %copy-done.2 = bf16[1,256,2048]{2,1,0:T(8,128)(2,1)S(1)} copy-done((bf16[1,256,2048]{2,1,0:T(8,128)(2,1)S(1)}, bf16[1,256,2048]{2,1,0:T(8,128)(2,1)}, u32[]{:S(2)}) %copy-start.2) | copy-done | bytes 1048600
  5.7 0.0 copy-start.3
  5.7 1.0 %copy-done.3 = bf16[128,2048]{1,0:T(8,128)(2,1)S(1)} copy-done((bf16[128,2048]{1,0:T(8,128)(2,1)S(1)}, bf16[128,2048]{1,0:T(8,128)(2,1)}, u32[]{:S(2)}) %copy-start.3) | copy-done | bytes 524312
  6.8 73.7 %expert_layer.1 = bf16[128,2048]{1,0:T(8,128)(2,1)S(1)} custom-call(bf16[128,2048]{1,0:T(8,128)(2,1)S(1)} %copy-done.3, f32[1,2048]{1,0:T(1,128)S(1)} %bitcast.1, s32[128,2]{1,0:T(8,128)S(1)} %copy.8.ids_ref, f32[128,2]{1,0:T(8,128)S(1)} %copy.9.gates_ref, bf16[1,2048,256]{2,1,0:T(8,128)(2,1)S(1)} %copy-done, bf16[1,2048,256]{2,1,0:T(8,128)(2,1)S(1)} %copy-done.1, ...), custom_call_target="tpu_custom_call" | custom-call | tf_op jit(solution)/shard_map/expert_layer/pallas_call | solution.py:328
  80.5 0.8 copy.11
Async XLA Ops:
  0.0 0.7 copy-start.5
  0.7 0.7 copy-start.6
  1.4 0.7 copy-start.4
  2.1 1.2 %copy-start = (bf16[1,2048,256]{2,1,0:T(8,128)(2,1)S(1)}, bf16[1,2048,256]{2,1,0:T(8,128)(2,1)}, u32[]{:S(2)}) copy-start(bf16[1,2048,256]{2,1,0:T(8,128)(2,1)} %gate_hbm.1) | copy-start | bytes 3145732
  3.3 1.2 %copy-start.1 = (bf16[1,2048,256]{2,1,0:T(8,128)(2,1)S(1)}, bf16[1,2048,256]{2,1,0:T(8,128)(2,1)}, u32[]{:S(2)}) copy-start(bf16[1,2048,256]{2,1,0:T(8,128)(2,1)} %up_hbm.1) | copy-start | bytes 3145732
  4.5 1.2 %copy-start.2 = (bf16[1,256,2048]{2,1,0:T(8,128)(2,1)S(1)}, bf16[1,256,2048]{2,1,0:T(8,128)(2,1)}, u32[]{:S(2)}) copy-start(bf16[1,256,2048]{2,1,0:T(8,128)(2,1)} %down_hbm.1) | copy-start | bytes 3145732
  5.7 1.0 %copy-start.3 = (bf16[128,2048]{1,0:T(8,128)(2,1)S(1)}, bf16[128,2048]{1,0:T(8,128)(2,1)}, u32[]{:S(2)}) copy-start(bf16[128,2048]{1,0:T(8,128)(2,1)} %tok_ref.1) | copy-start | bytes 1572868

commit v2 on v0

--- a/solution.py
+++ b/solution.py
@@ -1,6 +1,10 @@
+import functools
+
 import jax
 import jax.numpy as jnp
 from jax import lax
+from jax.experimental import pallas as pl
+from jax.experimental.pallas import tpu as pltpu
 from jax.sharding import PartitionSpec as P
 
 N_GROUPS = 4
@@ -32,7 +36,7 @@
     return total.astype(jnp.bfloat16)
 
 
-def shards(tokens, norm_gain, expert_ids, gate_weights, w_gate, w_up, w_down):
+def generic_shards(tokens, norm_gain, expert_ids, gate_weights, w_gate, w_up, w_down):
     normed = normalize(tokens, norm_gain)
     n_tok, model_width = normed.shape
     top_count = expert_ids.shape[1]
@@ -76,6 +80,293 @@
     return mixed.astype(jnp.bfloat16)
 
 
+LANES = 128
+MESH = pl.DeviceIdType.MESH
+
+
+def route_order(n_groups, home):
+    low = (home < n_groups // 2).astype(jnp.int32)
+    rim = low * home + (1 - low) * (n_groups - 1 - home)
+    order = [home]
+    for index in range(n_groups - 1):
+        inner = (index < 2 * rim).astype(jnp.int32)
+        step = index // 2 + 1 if index % 2 == 0 else -(index // 2 + 1)
+        at = inner * (rim + step) + (1 - inner) * (index + 1)
+        order.append(low * at + (1 - low) * (n_groups - 1 - at))
+    return order
+
+
+def layer_kernel(
+    n_groups, rows, tok_hbm, gain_ref, ids_ref, gates_ref, gate_hbm, up_hbm, down_hbm, out_ref,
+    tok, pick_ref, sent, inbox, own, other, from_pair, back, final, gate_w, up_w, down_w, place,
+    local_sem, w_send, w_recv, z_send, z_recv, y_send, y_recv, p_send, p_recv, b_send, b_recv,
+):
+    n_tok, width = tok.shape
+    members = 2
+    pieces = 2
+    cut = rows // pieces
+    ep = lax.axis_index("ep")
+    core = lax.axis_index("tp")
+    home = ep // members
+    member = ep % members
+    pair_id = {"ep": home * members + 1 - member}
+    core_id = {"tp": 1 - core}
+    order = route_order(n_groups, home)
+    at_end = jnp.logical_or(home == 0, home == n_groups - 1)
+
+    def row_id(group):
+        return {"ep": group * members + member}
+
+    def remote(src, dst, send, recv, target):
+        return pltpu.make_async_remote_copy(
+            src_ref=src, dst_ref=dst, send_sem=send, recv_sem=recv,
+            device_id=target, device_id_type=MESH,
+        )
+
+    tok_copy = pltpu.make_async_copy(tok_hbm, tok, local_sem.at[3])
+    tok_copy.start()
+    barrier = pltpu.get_barrier_semaphore()
+    for group in order[1:]:
+        pl.semaphore_signal(barrier, inc=1, device_id=row_id(group), device_id_type=MESH)
+    pl.semaphore_signal(barrier, inc=1, device_id=pair_id, device_id_type=MESH)
+    pl.semaphore_signal(barrier, inc=1, device_id=core_id, device_id_type=MESH)
+    weights = ((gate_hbm, gate_w), (up_hbm, up_w), (down_hbm, down_w))
+    loads = [
+        pltpu.make_async_copy(src.at[0], dst.at[core], local_sem.at[index])
+        for index, (src, dst) in enumerate(weights)
+    ]
+    for copy in loads:
+        copy.start()
+
+    token = lax.broadcasted_iota(jnp.int32, (n_tok, n_tok), 0)
+    lane = lax.broadcasted_iota(jnp.int32, (n_tok, n_tok), 1)
+    eye = token == lane
+
+    def column(row):
+        return jnp.sum(jnp.where(eye, row, jnp.zeros_like(row)), axis=1, keepdims=True)
+
+    first_id = ids_ref[0:1, :]
+    group_row = first_id // members
+    group_of = column(group_row)
+    onehot = (group_of == lane).astype(jnp.float32)
+    earlier = (token > lane).astype(jnp.bfloat16)
+    before = jnp.dot(earlier, onehot.astype(jnp.bfloat16), preferred_element_type=jnp.float32)
+    rank = jnp.sum(before * onehot, axis=1, keepdims=True).astype(jnp.int32)
+    slot = group_of * rows + rank
+    slots = lax.broadcasted_iota(jnp.int32, (n_tok, n_groups * rows), 1)
+    place_t = (slot == slots).astype(jnp.float32)
+    place[...] = place_t.astype(jnp.bfloat16)
+    pick_ref[...] = place_t.T.astype(jnp.bfloat16).reshape(pick_ref.shape)
+
+    first = (first_id % members) == 0
+    by_member = (
+        jnp.where(first, gates_ref[0:1, :], gates_ref[1:2, :]),
+        jnp.where(first, gates_ref[1:2, :], gates_ref[0:1, :]),
+    )
+    extra_lane = lax.broadcasted_iota(jnp.int32, (n_tok, LANES), 1)
+    extra = jnp.zeros((n_tok, LANES), jnp.float32)
+    for index, weight in enumerate(by_member):
+        left = column(weight)
+        for piece in range(3):
+            part = left.astype(jnp.bfloat16).astype(jnp.float32)
+            extra = jnp.where(extra_lane == index * 3 + piece, part, extra)
+            left = left - part
+    extra = extra.astype(jnp.bfloat16)
+
+    tok_copy.wait()
+    values = tok[...].astype(jnp.float32)
+    scale = lax.rsqrt(jnp.mean(values * values, axis=-1, keepdims=True) + 1e-06)
+    normed = (values * scale * gain_ref[...]).astype(jnp.bfloat16)
+
+    def bucket(index):
+        chosen = pick_ref[order[index]]
+        main = jnp.dot(chosen, normed, preferred_element_type=jnp.float32).astype(jnp.bfloat16)
+        side = jnp.dot(chosen, extra, preferred_element_type=jnp.float32).astype(jnp.bfloat16)
+        if index == 0:
+            inbox[home, 0:rows, :width] = main
+            inbox[home, 0:rows, width:] = side
+        else:
+            sent[index - 1, :, :width] = main
+            sent[index - 1, :, width:] = side
+
+    def z_copy(index, piece, source=None):
+        source = home if source is None else source
+        return remote(
+            sent.at[index - 1, pl.ds(piece * cut, cut)],
+            inbox.at[source, pl.ds(piece * cut, cut)],
+            z_send.at[index, piece],
+            z_recv.at[source, piece],
+            row_id(order[index]),
+        )
+
+    def y_copy(index, piece):
+        return remote(
+            inbox.at[order[index], pl.ds(piece * cut, cut)],
+            inbox.at[order[index], pl.ds(rows + piece * cut, cut)],
+            y_send.at[index, piece],
+            y_recv.at[index, piece],
+            pair_id,
+        )
+
+    def pair_copy(index, piece):
+        return remote(
+            other.at[index, pl.ds(piece * cut, cut)],
+            from_pair.at[index, pl.ds(piece * cut, cut)],
+            p_send.at[index, piece],
+            p_recv.at[index, piece],
+            pair_id,
+        )
+
+    def back_copy(index, piece, source=None):
+        source = home if source is None else source
+        return remote(
+            back.at[index, pl.ds(piece * cut, cut)],
+            final.at[source, pl.ds(piece * cut, cut)],
+            b_send.at[index, piece],
+            b_recv.at[source, piece],
+            row_id(order[index]),
+        )
+
+    pl.semaphore_wait(barrier, n_groups + 1)
+    shared = [
+        remote(src.at[0], dst.at[core], w_send.at[index], w_recv.at[index], core_id)
+        for index, (src, dst) in enumerate(weights)
+    ]
+    for copy in shared:
+        copy.start()
+    for index in (1, 0) + tuple(range(2, n_groups)):
+        bucket(index)
+        for piece in range(pieces):
+            (z_copy(index, piece) if index else y_copy(0, piece)).start()
+    for copy in loads:
+        copy.wait()
+    for copy in shared:
+        copy.wait()
+
+    def forward(index):
+        for piece in range(pieces):
+            z_copy(index, piece, order[index]).wait_recv()
+            y_copy(index, piece).start()
+
+    def compute(index):
+        for piece in range(pieces):
+            y_copy(index, piece).wait_recv()
+        group = order[index]
+        x = inbox[group, :, :width]
+        tail = inbox[group, :, width:].astype(jnp.float32)
+        by_expert = [
+            tail[:, k : k + 1] + tail[:, k + 1 : k + 2] + tail[:, k + 2 : k + 3] for k in (0, 3)
+        ]
+        weight = jnp.where(member == 0, by_expert[0], by_expert[1])
+        hidden = []
+        for j in range(2):
+            g = jnp.dot(x, gate_w[j], preferred_element_type=jnp.float32)
+            u = jnp.dot(x, up_w[j], preferred_element_type=jnp.float32)
+            hidden.append((g / (1.0 + jnp.exp(-g)) * u).astype(jnp.bfloat16))
+        step = min(512, width)
+        for begin in range(0, width, step):
+            out = jnp.dot(
+                hidden[0], down_w[0, :, begin : begin + step], preferred_element_type=jnp.float32
+            ) + jnp.dot(
+                hidden[1], down_w[1, :, begin : begin + step], preferred_element_type=jnp.float32
+            )
+            out = out * weight
+            own[index, :, begin : begin + step] = out[:rows]
+            other[index, :, begin : begin + step] = out[rows:].astype(jnp.bfloat16)
+
+    def give(index):
+        for piece in range(pieces):
+            pair_copy(index, piece).start()
+
+    def combine(index):
+        for piece in range(pieces):
+            pair_copy(index, piece).wait_recv()
+            at = slice(piece * cut, (piece + 1) * cut)
+            total = own[index, at] + from_pair[index, at].astype(jnp.float32)
+            total = total.astype(jnp.bfloat16)
+            if index == 0:
+                final[home, at] = total
+            else:
+                back[index, at] = total
+                back_copy(index, piece).start()
+
+    last = n_groups - 1
+    forward(1)
+    if last > 2:
+        pl.when(jnp.logical_not(at_end))(lambda: forward(2))
+    compute(0)
+    compute(1)
+    give(1)
+    if last > 2:
+        pl.when(at_end)(lambda: forward(2))
+    for index in range(3 if last > 2 else 2, n_groups):
+        forward(index)
+    combine(1)
+    for index in range(2, n_groups):
+        compute(index)
+        give(index)
+    give(0)
+    for index in range(2, n_groups):
+        combine(index)
+    combine(0)
+    for index in range(1, n_groups):
+        for piece in range(pieces):
+            back_copy(index, piece, order[index]).wait_recv()
+    mixed = jnp.dot(
+        place[...], final[...].reshape(n_groups * rows, width), preferred_element_type=jnp.float32
+    )
+    out_ref[...] = mixed.astype(out_ref.dtype)
+    for index in range(n_groups):
+        for piece in range(pieces):
+            if index:
+                z_copy(index, piece).wait_send()
+                back_copy(index, piece).wait_send()
+            y_copy(index, piece).wait_send()
+            pair_copy(index, piece).wait_send()
+
+
+def shards(tokens, norm_gain, expert_ids, gate_weights, w_gate, w_up, w_down):
+    n_tok, width = tokens.shape
+    local_experts = w_gate.shape[0]
+    n_exp = local_experts * lax.axis_size("ep")
+    per_group = n_exp // N_GROUPS
+    top_count = expert_ids.shape[1]
+    if not (local_experts == 1 and per_group == 2 and top_count == 2 and lax.axis_size("tp") == 2):
+        return generic_shards(tokens, norm_gain, expert_ids, gate_weights, w_gate, w_up, w_down)
+    rows = n_tok // 2
+    half = w_gate.shape[2]
+    bf16, f32 = jnp.bfloat16, jnp.float32
+    dma = pltpu.SemaphoreType.DMA
+    vmem = pl.BlockSpec(memory_space=pltpu.VMEM)
+    hbm = pl.BlockSpec(memory_space=pl.ANY)
+    return pl.pallas_call(
+        functools.partial(layer_kernel, N_GROUPS, rows),
+        out_shape=jax.ShapeDtypeStruct((n_tok, width), bf16),
+        in_specs=[hbm] + [vmem] * 3 + [hbm] * 3,
+        out_specs=vmem,
+        scratch_shapes=[
+            pltpu.VMEM((n_tok, width), bf16),
+            pltpu.VMEM((N_GROUPS, rows, n_tok), bf16),
+            pltpu.VMEM((N_GROUPS - 1, rows, width + LANES), bf16),
+            pltpu.VMEM((N_GROUPS, 2 * rows, width + LANES), bf16),
+            pltpu.VMEM((N_GROUPS, rows, width), f32),
+            pltpu.VMEM((N_GROUPS, rows, width), bf16),
+            pltpu.VMEM((N_GROUPS, rows, width), bf16),
+            pltpu.VMEM((N_GROUPS, rows, width), bf16),
+            pltpu.VMEM((N_GROUPS, rows, width), bf16),
+            pltpu.VMEM((2, width, half), bf16),
+            pltpu.VMEM((2, width, half), bf16),
+            pltpu.VMEM((2, half, width), bf16),
+            pltpu.VMEM((n_tok, N_GROUPS * rows), bf16),
+            dma((4,)), dma((3,)), dma((3,)),
+        ] + [dma((N_GROUPS, 2))] * 8,
+        compiler_params=pltpu.CompilerParams(
+            collective_id=0, has_side_effects=True, vmem_limit_bytes=67043328
+        ),
+        name="expert_layer",
+    )(tokens, norm_gain.reshape(1, width), expert_ids.T, gate_weights.T, w_gate, w_up, w_down)
+
+
 def solution(mesh):
     placed = (
         P(("grp", "ep", "tp"), None),

time: 142 us -> 66.6 us (0.47)
  waiting for transfers between devices: 97.2 us -> 0 us
  Pallas kernels: 0 us -> 64.5 us
  matrix products: 14.7 us -> 0 us
  between operations: 13.2 us -> 0.01 us
  starting transfers between devices: 11.1 us -> 0 us
  other arithmetic: 4.17 us -> 0 us
    all_to_all x2 -> x0, waiting for transfers between devices: 95.1 us -> none  [the longest x1 48.4 us: shards(): lax.all_to_all(computed, 'ep', split_axis=0, concat_axis=0, tiled=True)]
    pallas_call x0 -> x1, Pallas kernels: none -> 64.5 us  [shards(): pl.pallas_call(functools.partial(layer_kernel, N_GROUPS, rows), out_shape...]
    dot_general x8 -> x0, matrix products: 14.7 us -> none  [the longest x1 3.84 us: expert_whole(): jnp.einsum('secd,edf->secf', bucket_rows, full_gate, preferred_element_ty...]
    all_to_all x2 -> x0, starting transfers between devices: 11.1 us -> none  [the longest x1 7.31 us: shards(): lax.all_to_all(buckets, 'ep', split_axis=0, concat_axis=0, tiled=True)]
    reshape x1 -> x0, other arithmetic: 2.16 us -> none  [shards(): expert_whole(grouped_rows, full_gate, full_up, full_down, n_tp)]
    unnamed x3 -> x0, waiting for transfers between devices: 2.09 us -> none
  transfers between devices with their start and end apart: 5 -> 0, of which waited for: 2 -> 0; matrix products, arithmetic and copies ran while one was open for 9% -> 0% of each run, Pallas kernels for 0% -> 0%
where the time goes in v2:
time: 66.6 us; the launch traced here: 66.4 us
  Pallas kernels  64.5 us (97%)
  local copies, waits for them, and re-layouts  1.88 us (3%)
    pallas_call x1, Pallas kernels, shards(): pl.pallas_call(functools.partial(layer_kernel, N_GROUPS, rows), out_shape...  64.5 us
    unnamed x1, local copies, waits for them, and re-layouts  1.88 us

profile of v2, /device:TPU:0, one launch (start us, length us, event | category | flops | bytes accessed | tf_op | source)
XLA Modules:
  0.0 66.4 jit_solution(14854339714842410781)
XLA Ops:
  0.0 64.5 %expert_layer.1 = bf16[128,2048]{1,0:T(8,128)(2,1)} custom-call(bf16[128,2048]{1,0:T(8,128)(2,1)} %tok_hbm.1, f32[1,2048]{1,0:T(1,128)} %bitcast.3, s32[2,128]{1,0:T(2,128)} %bitcast.4, f32[2,128]{1,0:T(2,128)} %bitcast.5, bf16[1,2048,256]{2,1,0:T(8,128)(2,1)} %gate_hbm.1, bf16[1,2048,256]{2,1,0:T(8,128)(2,1)} %up_hbm.1, bf16[1,256,2048]{2,1,0:T(8,128)(2,1)} %down_hbm.1), custom_call_target="tpu_custom_call" | custom-call | tf_op jit(solution)/shard_map/expert_layer/pallas_call | solution.py:342
  64.5 1.9 %copy.9 = bf16[128,2048]{1,0:T(8,128)(2,1)} copy(bf16[128,2048]{1,0:T(8,128)(2,1)} %expert_layer.1) | data formatting | bytes 1048576

commit v3 on v2

--- a/solution.py
+++ b/solution.py
@@ -103,7 +103,7 @@
 ):
     n_tok, width = tok.shape
     members = 2
-    pieces = 2
+    pieces = 4
     cut = rows // pieces
     ep = lax.axis_index("ep")
     core = lax.axis_index("tp")
@@ -359,7 +359,7 @@
             pltpu.VMEM((2, half, width), bf16),
             pltpu.VMEM((n_tok, N_GROUPS * rows), bf16),
             dma((4,)), dma((3,)), dma((3,)),
-        ] + [dma((N_GROUPS, 2))] * 8,
+        ] + [dma((N_GROUPS, 4))] * 8,
         compiler_params=pltpu.CompilerParams(
             collective_id=0, has_side_effects=True, vmem_limit_bytes=67043328
         ),

time: 66.6 us -> 65.4 us (0.982)
  Pallas kernels: 64.5 us -> 63.3 us
    pallas_call x1, Pallas kernels: 64.5 us -> 63.3 us  [shards(): pl.pallas_call(functools.partial(layer_kernel, N_GROUPS, rows), out_shape...]
where the time goes in v3:
time: 65.4 us; the launch traced here: 65.2 us
  Pallas kernels  63.3 us (97%)
  local copies, waits for them, and re-layouts  1.88 us (3%)
    pallas_call x1, Pallas kernels, shards(): pl.pallas_call(functools.partial(layer_kernel, N_GROUPS, rows), out_shape...  63.3 us
    unnamed x1, local copies, waits for them, and re-layouts  1.88 us

profile of v3, /device:TPU:0, one launch (start us, length us, event | category | flops | bytes accessed | tf_op | source)
XLA Modules:
  0.0 65.2 jit_solution(7594575377295074477)
XLA Ops:
  0.0 63.3 %expert_layer.1 = bf16[128,2048]{1,0:T(8,128)(2,1)} custom-call(bf16[128,2048]{1,0:T(8,128)(2,1)} %tok_hbm.1, f32[1,2048]{1,0:T(1,128)} %bitcast.3, s32[2,128]{1,0:T(2,128)} %bitcast.4, f32[2,128]{1,0:T(2,128)} %bitcast.5, bf16[1,2048,256]{2,1,0:T(8,128)(2,1)} %gate_hbm.1, bf16[1,2048,256]{2,1,0:T(8,128)(2,1)} %up_hbm.1, bf16[1,256,2048]{2,1,0:T(8,128)(2,1)} %down_hbm.1), custom_call_target="tpu_custom_call" | custom-call | tf_op jit(solution)/shard_map/expert_layer/pallas_call | solution.py:342
  63.3 1.9 %copy.9 = bf16[128,2048]{1,0:T(8,128)(2,1)} copy(bf16[128,2048]{1,0:T(8,128)(2,1)} %expert_layer.1) | data formatting | bytes 1048576
